TPU v7x, 32 devices: a whole 2x2x4 slice. The times are simulated.
32 devices in a mesh: fs: 8 (over z, y), tp: 4 (over x, core).
Axes of the slice: x: 2, y: 2, z: 4, core: 2. Of those that a mesh axis runs over, the one named last changes fastest.
Arguments:
- hidden_in: bfloat16 [512, 4096], P(None, 'tp'), may hold values from -6 to 6
- up_act: bfloat16 [512, 12288], P('tp', 'fs'), may hold values from -6 to 6
- up_val: bfloat16 [512, 12288], P('tp', 'fs'), may hold values from -6 to 6
- cotangent: bfloat16 [512, 4096], P('tp'), may hold values from -6 to 6
- w_act: bfloat16 [4096, 12288], P('tp', 'fs'), may hold values from -0.09375 to 0.09375
- w_val: bfloat16 [4096, 12288], P('tp', 'fs'), may hold values from -0.09375 to 0.09375
- w_down: bfloat16 [12288, 4096], P('fs', 'tp'), may hold values from -0.0546875 to 0.0546875
- conv_act: bfloat16 [3, 12288], P(None, 'fs'), may hold values from -3 to 3
- conv_val: bfloat16 [3, 12288], P(None, 'fs'), may hold values from -3 to 3
- bias_act: bfloat16 [12288], P('fs'), may hold values from -3 to 3
- bias_val: bfloat16 [12288], P('fs'), may hold values from -3 to 3
Outputs:
- grad_input: bfloat16 [512, 4096], P(('tp', 'fs'))
- grad_w_act: float32 [4096, 12288], P('tp', 'fs')
- grad_w_val: float32 [4096, 12288], P('tp', 'fs')
- grad_w_down: float32 [12288, 4096], P('fs', 'tp')
- grad_conv_act: float32 [3, 12288], P(None, 'fs')
- grad_conv_val: float32 [3, 12288], P(None, 'fs')
- grad_bias_act: float32 [12288], P('fs')
- grad_bias_val: float32 [12288], P('fs')
- rows_act: float32 [4096], P('tp')
- rows_val: float32 [4096], P('tp')
- rows_down: float32 [12288], P('fs')
- conv_rows: float32 [2, 3], replicated
All inputs are finite; a program needn't handle non-finite values.
Results may differ from a plain program's by a relative error of at most 0.0057.
Values may be sent and summed in bfloat16 or wider, within the bound.
No kernel may reach another device: no remote copies, remote signals or barrier semaphores. Data moves between devices by JAX's collectives and lax.ppermute only.
A program may use at most 128 MiB of HBM per device.

v0:
```python
import jax
import jax.numpy as jnp
from jax import lax
from jax.sharding import PartitionSpec as P


def passed_along(value, axis, by):
    length = lax.axis_size(axis)
    pairs = [(i, i + by) for i in range(length) if 0 <= i + by < length]
    return lax.ppermute(value, axis, pairs)


def contract_last(left, right):
    return lax.dot_general(
        left, right, (((1,), (1,)), ((), ())), preferred_element_type=jnp.float32
    )


def contract_first(left, right):
    return lax.dot_general(
        left, right, (((0,), (0,)), ((), ())), preferred_element_type=jnp.float32
    )


def conv_ahead(extended, taps, bias, length):
    total = jnp.zeros((length, extended.shape[1]), jnp.float32) + bias.astype(jnp.float32)
    for offset in range(taps.shape[0]):
        total = total + taps[offset].astype(jnp.float32) * extended[offset : offset + length]
    return total


def conv_behind(extended, taps, length):
    reach = taps.shape[0] - 1
    total = jnp.zeros((length, extended.shape[1]), jnp.float32)
    for offset in range(taps.shape[0]):
        total = (
            total
            + taps[offset].astype(jnp.float32) * extended[reach - offset : reach - offset + length]
        )
    return total.astype(jnp.bfloat16)


def tap_grads(grad_pre, extended, tap_count):
    length = grad_pre.shape[0]
    rows = [
        jnp.sum(grad_pre * extended[offset : offset + length], axis=0)
        for offset in range(tap_count)
    ]
    return (jnp.stack(rows, 0), jnp.sum(grad_pre, axis=0))


def per_device(
    hidden_in,
    up_act,
    up_val,
    cotangent,
    w_act,
    w_val,
    w_down,
    conv_act,
    conv_val,
    bias_act,
    bias_val,
):
    local_rows = cotangent.shape[0]
    tap_count = conv_act.shape[0]
    reach = tap_count - 1
    tp_count = lax.axis_size("tp")
    fs_count = lax.axis_size("fs")
    down_whole = lax.all_gather(w_down, "tp", axis=1, tiled=True)
    prev_act, prev_val = passed_along(
        (up_act[local_rows - reach :], up_val[local_rows - reach :]), "tp", 1
    )
    ext_act = jnp.concatenate([prev_act, up_act], 0).astype(jnp.float32)
    ext_val = jnp.concatenate([prev_val, up_val], 0).astype(jnp.float32)
    pre_act = conv_ahead(ext_act, conv_act, bias_act, local_rows)
    pre_val = conv_ahead(ext_val, conv_val, bias_val, local_rows)
    gelu_act, gelu_back = jax.vjp(jax.nn.gelu, pre_act)
    mixed = (gelu_act * pre_val).astype(jnp.bfloat16)
    grad_mixed = contract_last(cotangent, down_whole).astype(jnp.bfloat16)
    grad_mixed = lax.optimization_barrier(grad_mixed).astype(jnp.float32)
    grad_pre_act = gelu_back(grad_mixed * pre_val)[0]
    grad_pre_val = grad_mixed * gelu_act
    next_act, next_val = passed_along((grad_pre_act[:reach], grad_pre_val[:reach]), "tp", -1)
    grad_up_act = conv_behind(jnp.concatenate([grad_pre_act, next_act], 0), conv_act, local_rows)
    grad_up_val = conv_behind(jnp.concatenate([grad_pre_val, next_val], 0), conv_val, local_rows)
    taps_act, sums_act = tap_grads(grad_pre_act, ext_act, tap_count)
    taps_val, sums_val = tap_grads(grad_pre_val, ext_val, tap_count)
    all_up_act, all_up_val, all_mixed = (
        lax.all_gather(grad_up_act, "tp", axis=0, tiled=True),
        lax.all_gather(grad_up_val, "tp", axis=0, tiled=True),
        lax.all_gather(mixed, "tp", axis=0, tiled=True),
    )
    cot_columns = lax.all_to_all(cotangent, "tp", split_axis=1, concat_axis=0, tiled=True)
    grad_w_act = contract_first(hidden_in, all_up_act)
    grad_w_val = contract_first(hidden_in, all_up_val)
    grad_w_down = contract_first(all_mixed, cot_columns)
    shard_rows = local_rows // fs_count
    block_rows = tp_count * shard_rows

    def select_rows(gathered):
        shaped = gathered.reshape(tp_count, fs_count, shard_rows, gathered.shape[1])
        return jnp.transpose(shaped, (1, 0, 2, 3)).reshape(
            lax.axis_size("fs") * block_rows, gathered.shape[1]
        )

    summed = lax.psum_scatter(
        contract_last(select_rows(all_up_act), w_act)
        + contract_last(select_rows(all_up_val), w_val),
        "fs",
        scatter_dimension=0,
        tiled=True,
    ).astype(jnp.bfloat16)
    grad_input = lax.all_to_all(summed, "tp", split_axis=0, concat_axis=1, tiled=True)
    down_squares = jnp.sum(grad_w_down * grad_w_down, axis=1)
    taps_act, taps_val, sums_act, sums_val, rows_down = lax.psum(
        (taps_act, taps_val, sums_act, sums_val, down_squares), "tp"
    )
    tap_squares = jnp.stack(
        [jnp.sum(taps_act * taps_act, axis=1), jnp.sum(taps_val * taps_val, axis=1)], 0
    )
    rows_act, rows_val, conv_rows = lax.psum(
        (
            jnp.sum(grad_w_act * grad_w_act, axis=1),
            jnp.sum(grad_w_val * grad_w_val, axis=1),
            tap_squares,
        ),
        "fs",
    )
    return (
        grad_input,
        grad_w_act,
        grad_w_val,
        grad_w_down,
        taps_act,
        taps_val,
        sums_act,
        sums_val,
        rows_act,
        rows_val,
        rows_down,
        conv_rows,
    )


def solution(mesh):
    return jax.shard_map(
        per_device,
        mesh=mesh,
        in_specs=(
            P(None, "tp"),
            P("tp", "fs"),
            P("tp", "fs"),
            P("tp", None),
            P("tp", "fs"),
            P("tp", "fs"),
            P("fs", "tp"),
            P(None, "fs"),
            P(None, "fs"),
            P("fs"),
            P("fs"),
        ),
        out_specs=(
            P(("tp", "fs"), None),
            P("tp", "fs"),
            P("tp", "fs"),
            P("fs", "tp"),
            P(None, "fs"),
            P(None, "fs"),
            P("fs"),
            P("fs"),
            P("tp"),
            P("tp"),
            P("fs"),
            P(),
        ),
        check_vma=False,
    )
```

profile of v0, /device:TPU:0, one launch (start us, length us, event | category | flops | bytes accessed | tf_op | source)
XLA Modules:
  0.0 296.1 jit_solution(9692622403794457745)
XLA Ops:
  8.4 2.4 collective-permute-start.1
  11.5 4.5 %collective-permute-start = (bf16[2,1536]{1,0:T(2,128)(2,1)S(1)}, bf16[2,1536]{1,0:T(2,128)(2,1)S(1)}, u32[]{:S(2)}, u32[]{:S(2)}) collective-permute-start(bf16[2,1536]{1,0:T(2,128)(2,1)S(1)} %slice.74), channel_id=1, source_target_pairs={{0,1},{1,2},{2,3},{4,5},{5,6},{6,7},{8,9},{9,10},{10,11},{12,13},{... | collective-permute-start | bytes 18440 | tf_op jit(solution)/shard_map/ppermute | solution.py:10
  19.8 2.1 maximum_convert_fusion
  21.9 72.5 %all-gather.5.cloned.1.call-done = bf16[1536,4096]{1,0:T(8,128)(2,1)} async-done(((bf16[1536,1024]{1,0:T(8,128)(2,1)}), bf16[1536,4096]{1,0:T(8,128)(2,1)}) %all-gather.5.cloned.1.call-update) | async-done | bytes 12582928 | tf_op jit(solution)/shard_map/all_gather | solution.py:70
  94.4 9.3 %convolution_convert_fusion = bf16[128,1536]{1,0:T(8,128)(2,1)S(1)} fusion(bf16[128,4096]{1,0:T(8,128)(2,1)} %param.14, bf16[1536,4096]{1,0:T(8,128)(2,1)} %all-gather.5.cloned.1.call-done), kind=kOutput, calls=%fused_computation.5 | convolution fusion | flops 1610809344 | bytes 14024704 | tf_op jit(solution)/shard_map/dot_general | solution.py:14
  107.8 2.1 multiply_reduce_fusion.8
  112.1 3.5 %collective-permute-done.2 = f32[2,1536]{1,0:T(2,128)S(1)} collective-permute-done((f32[2,1536]{1,0:T(2,128)S(1)}, f32[2,1536]{1,0:T(2,128)S(1)}, u32[]{:S(2)}, u32[]{:S(2)}) %collective-permute-start.2) | collective-permute-done | bytes 12320 | tf_op jit(solution)/shard_map/ppermute | solution.py:10
  115.5 3.0 fusion.9
  118.6 2.5 multiply_convert_fusion
  121.2 10.4 %all-gather.9.cloned.1.call-done = bf16[512,1536]{1,0:T(8,128)(2,1)} async-done(((bf16[128,1536]{1,0:T(8,128)(2,1)}), bf16[512,1536]{1,0:T(8,128)(2,1)}) %all-gather.9.cloned.1.call-update) | async-done | bytes 1572880 | tf_op jit(solution)/shard_map/all_gather | solution.py:91
  131.5 2.7 copy.34
  134.2 18.6 %all-gather.7.cloned.1.call-done = bf16[512,1536]{1,0:T(8,128)(2,1)} async-done(((bf16[128,1536]{1,0:T(8,128)(2,1)}), bf16[512,1536]{1,0:T(8,128)(2,1)}) %all-gather.7.cloned.1.call-update) | async-done | bytes 1572880 | tf_op jit(solution)/shard_map/all_gather | solution.py:90
  156.7 3.2 %convolution_add_fusion = f32[512,1024]{1,0:T(8,128)} fusion(f32[512,1024]{1,0:T(8,128)S(1)} %fusion.19, bf16[512,1536]{1,0:T(8,128)(2,1)S(1)} %bitcast.37, bf16[1024,1536]{1,0:T(8,128)(2,1)S(1)} %copy-done.17), kind=kOutput, calls=%fused_computation.6 | convolution fusion | flops 1611137024 | bytes 8912896 | tf_op jit(solution)/shard_map/dot_general | solution.py:14
  161.8 21.8 %all_to_all.38 = bf16[128,4,1024]{0,2,1:T(8,128)(2,1)S(1)} all-to-all(bf16[128,4,1024]{0,2,1:T(8,128)(2,1)S(1)} %bitcast.34), channel_id=1, replica_groups=mesh['fs'=8,'tp'=4] {'tp'}, dimensions={1} | all-to-all | bytes 2097152 | tf_op jit(solution)/shard_map/all_to_all | solution.py:94
  185.4 5.8 %multiply_reduce_fusion.1 = (f32[1024]{0:T(1024)S(1)}, f32[1024,1536]{0,1:T(8,128)}) fusion(bf16[512,1536]{1,0:T(8,128)(2,1)S(1)} %copy-done.7, bf16[512,1024]{1,0:T(8,128)(2,1)} %param.11), kind=kOutput, calls=%fused_computation.1 | convolution fusion | flops 1613757440 | bytes 8916992 | tf_op jit(solution)/shard_map/dot_general | solution.py:20
  191.1 6.7 %copy.39 = f32[1024,1536]{1,0:T(8,128)} copy(f32[1024,1536]{0,1:T(8,128)} %get-tuple-element.80) | data formatting | bytes 12582912
  197.8 6.0 %multiply_reduce_fusion = (f32[1536]{0:T(1024)S(1)}, f32[1536,1024]{0,1:T(8,128)}) fusion(bf16[512,1536]{1,0:T(8,128)(2,1)} %all-gather.11.cloned.1.call-done, bf16[512,1024]{1,0:T(8,128)(2,1)S(1)} %bitcast.39), kind=kOutput, calls=%fused_computation | convolution fusion | flops 1613756928 | bytes 8919040 | tf_op jit(solution)/shard_map/dot_general | solution.py:20
  203.8 6.7 %copy.40 = f32[1536,1024]{1,0:T(8,128)} copy(f32[1536,1024]{0,1:T(8,128)} %get-tuple-element.76) | data formatting | bytes 12582912
  210.5 11.9 %all-reduce.1 = (f32[3,1536]{1,0:T(4,128)S(1)}, f32[3,1536]{1,0:T(4,128)S(1)}, f32[1536]{0:T(1024)}, f32[1536]{0:T(1024)}, f32[1536]{0:T(1024)}) all-reduce(f32[3,1536]{1,0:T(4,128)S(1)} %pad_maximum_fusion.2, f32[3,1536]{1,0:T(4,128)S(1)} %pad_maximum_fusion.3, ...), channel_id=1, replica_groups=mesh['fs'=8,'tp'=4] {'tp'}, use_global_device_ids=true, to_apply=%region_4.0 | all-reduce | flops 13824 | bytes 110592 | tf_op jit(solution)/shard_map/psum | solution.py:116
  222.6 28.7 %reduce-scatter.2.cloned.1.call-done = f32[64,1024]{1,0:T(8,128)} async-done(((f32[512,1024]{1,0:T(8,128)}), f32[64,1024]{1,0:T(8,128)}) %reduce-scatter.2.cloned.1.call-update) | async-done | bytes 262160 | tf_op jit(solution)/shard_map/reduce_scatter | solution.py:107
  252.9 3.3 %all-to-all-start = ((bf16[4,16,1024]{2,1,0:T(8,128)(2,1)}), bf16[4,16,1024]{2,1,0:T(8,128)(2,1)S(1)}, u32[]{:S(2)}, u32[]{:S(2)}) async-start(bf16[4,16,1024]{2,1,0:T(8,128)(2,1)} %bitcast.6), calls=%async_computation.1 | async-start | bytes 262144 | tf_op jit(solution)/shard_map/all_to_all | solution.py:114
  256.3 5.7 %multiply_reduce_fusion.2 = (f32[1024]{0:T(1024)S(1)}, f32[1024,1536]{0,1:T(8,128)}) fusion(bf16[512,1536]{1,0:T(8,128)(2,1)S(1)} %copy-done.6, bf16[512,1024]{1,0:T(8,128)(2,1)} %param.11), kind=kOutput, calls=%fused_computation.2 | convolution fusion | flops 1613757440 | bytes 8916992 | tf_op jit(solution)/shard_map/dot_general | solution.py:20
  262.0 6.7 %copy.38 = f32[1024,1536]{1,0:T(8,128)} copy(f32[1024,1536]{0,1:T(8,128)} %get-tuple-element.78) | data formatting | bytes 12582912
  268.7 20.2 %all-reduce = (f32[1024]{0:T(1024)}, f32[1024]{0:T(1024)}, f32[2,3]{1,0:T(2,128)}) all-reduce(f32[1024]{0:T(1024)S(1)} %get-tuple-element.77, f32[1024]{0:T(1024)S(1)} %get-tuple-element.79, f32[2,3]{1,0:T(2,128)S(1)} %pad_maximum_fusion.4), channel_id=1, replica_groups=mesh['fs'=8,'tp'=4] {'fs'}, use_global_device_ids=true, to_apply=%region_14.0 | all-reduce | flops 2054 | bytes 16432 | tf_op jit(solution)/shard_map/psum | solution.py:122
  (79 shorter events, 21.9 us)
Async XLA Ops:
  7.2 147.1 %copy-start = (bf16[1024,1536]{1,0:T(8,128)(2,1)S(1)}, bf16[1024,1536]{1,0:T(8,128)(2,1)}, u32[]{:S(2)}) copy-start(bf16[1024,1536]{1,0:T(8,128)(2,1)} %param.15) | copy-start | bytes 9437188
  7.2 87.2 %all-gather.5.cloned.1.call-start = ((), (), s32[]{:S(2)}) async-start(), calls=%async_computation.3 | async-start | bytes 15728640 | tf_op jit(solution)/shard_map/all_gather | solution.py:70
  7.9 123.6 %all-gather.9.cloned.1.call-start = ((), (), s32[]{:S(2)}) async-start(), calls=%async_computation.5 | async-start | bytes 1966080 | tf_op jit(solution)/shard_map/all_gather | solution.py:91
  8.4 10.4 %collective-permute-start.1 = (bf16[2,1536]{1,0:T(2,128)(2,1)S(1)}, bf16[2,1536]{1,0:T(2,128)(2,1)S(1)}, u32[]{:S(2)}, u32[]{:S(2)}) collective-permute-start(bf16[2,1536]{1,0:T(2,128)(2,1)S(1)} %slice.80), channel_id=1, source_target_pairs={{0,1},{1,2},{2,3},{4,5},{5,6},{6,7},{8,9},{9,10},{10,11},{12,13},{... | collective-permute-start | bytes 18440 | tf_op jit(solution)/shard_map/ppermute | solution.py:10
  11.5 8.3 %collective-permute-start = (bf16[2,1536]{1,0:T(2,128)(2,1)S(1)}, bf16[2,1536]{1,0:T(2,128)(2,1)S(1)}, u32[]{:S(2)}, u32[]{:S(2)}) collective-permute-start(bf16[2,1536]{1,0:T(2,128)(2,1)S(1)} %slice.74), channel_id=1, source_target_pairs={{0,1},{1,2},{2,3},{4,5},{5,6},{6,7},{8,9},{9,10},{10,11},{12,13},{... | collective-permute-start | bytes 18440 | tf_op jit(solution)/shard_map/ppermute | solution.py:10
  21.9 81.8 %copy-start.11 = (f32[1536]{0:T(1024)S(1)}, f32[1536]{0:T(1024)}, u32[]{:S(2)}) copy-start(f32[1536]{0:T(1024)} %get-tuple-element.61) | copy-start | bytes 18436
  21.9 81.8 %copy-start.12 = (f32[1536]{0:T(1024)S(1)}, f32[1536]{0:T(1024)}, u32[]{:S(2)}) copy-start(f32[1536]{0:T(1024)} %convert_element_type.52) | copy-start | bytes 18436
  94.4 9.3 %copy-start.2 = (f32[130,1536]{1,0:T(8,128)S(1)}, f32[130,1536]{1,0:T(8,128)}, u32[]{:S(2)}) copy-start(f32[130,1536]{1,0:T(8,128)} %maximum_convert_fusion.1) | copy-start | bytes 2396164
  94.4 9.3 %copy-start.3 = (f32[130,1536]{1,0:T(8,128)S(1)}, f32[130,1536]{1,0:T(8,128)}, u32[]{:S(2)}) copy-start(f32[130,1536]{1,0:T(8,128)} %maximum_convert_fusion) | copy-start | bytes 2396164
  103.8 2.2 copy-start.13
  103.8 2.3 copy-start.16
  104.7 5.2 %copy-start.4 = (f32[128,1536]{1,0:T(8,128)}, f32[128,1536]{1,0:T(8,128)S(1)}, u32[]{:S(2)}) copy-start(f32[128,1536]{1,0:T(8,128)S(1)} %get-tuple-element.71) | copy-start | bytes 2359300
  104.7 3.1 %collective-permute-start.3 = (f32[2,1536]{1,0:T(2,128)S(1)}, f32[2,1536]{1,0:T(2,128)S(1)}, u32[]{:S(2)}, u32[]{:S(2)}) collective-permute-start(f32[2,1536]{1,0:T(2,128)S(1)} %slice.101), channel_id=1, source_target_pairs={{1,0},{2,1},{3,2},{5,4},{6,5},{7,6},{9,8},{10,9},{11,10},{13,12},{... | collective-permute-start | bytes 36872 | tf_op jit(solution)/shard_map/ppermute | solution.py:10
  109.9 42.9 %all-gather.7.cloned.1.call-start = ((), (), s32[]{:S(2)}) async-start(), calls=%async_computation.4 | async-start | bytes 1966080 | tf_op jit(solution)/shard_map/all_gather | solution.py:90
  110.8 4.8 %collective-permute-start.2 = (f32[2,1536]{1,0:T(2,128)S(1)}, f32[2,1536]{1,0:T(2,128)S(1)}, u32[]{:S(2)}, u32[]{:S(2)}) collective-permute-start(f32[2,1536]{1,0:T(2,128)S(1)} %slice.98), channel_id=1, source_target_pairs={{1,0},{2,1},{3,2},{5,4},{6,5},{7,6},{9,8},{10,9},{11,10},{13,12},{... | collective-permute-start | bytes 36872 | tf_op jit(solution)/shard_map/ppermute | solution.py:10
  118.5 79.3 %all-gather.11.cloned.1.call-start = ((), (), s32[]{:S(2)}) async-start(), calls=%async_computation.7 | async-start | bytes 1966080 | tf_op jit(solution)/shard_map/all_gather | solution.py:92
  121.1 130.2 %reduce-scatter.2.cloned.1.call-start = ((), (), s32[]{:S(2)}) async-start(), calls=%async_computation.6 | async-start | bytes 2359296 | tf_op jit(solution)/shard_map/reduce_scatter | solution.py:107
  154.3 2.4 copy-start.17
  191.1 6.7 %copy-start.9 = (bf16[4,128,1024]{2,1,0:T(8,128)(2,1)S(1)}, bf16[4,128,1024]{2,1,0:T(8,128)(2,1)}, u32[]{:S(2)}) copy-start(bf16[4,128,1024]{2,1,0:T(8,128)(2,1)} %copy.37) | copy-start | bytes 3145732
  203.8 52.5 %copy-start.6 = (bf16[512,1536]{1,0:T(8,128)(2,1)S(1)}, bf16[512,1536]{1,0:T(8,128)(2,1)}, u32[]{:S(2)}) copy-start(bf16[512,1536]{1,0:T(8,128)(2,1)} %all-gather.7.cloned.1.call-done) | copy-start | bytes 4718596
  222.4 39.5 %copy-start.14 = (f32[3,1536]{1,0:T(4,128)}, f32[3,1536]{1,0:T(4,128)S(1)}, u32[]{:S(2)}) copy-start(f32[3,1536]{1,0:T(4,128)S(1)} %get-tuple-element.65) | copy-start | bytes 55300
  222.4 39.5 %copy-start.15 = (f32[3,1536]{1,0:T(4,128)}, f32[3,1536]{1,0:T(4,128)S(1)}, u32[]{:S(2)}) copy-start(f32[3,1536]{1,0:T(4,128)S(1)} %get-tuple-element.66) | copy-start | bytes 55300
  252.9 35.9 %all-to-all-start = ((bf16[4,16,1024]{2,1,0:T(8,128)(2,1)}), bf16[4,16,1024]{2,1,0:T(8,128)(2,1)S(1)}, u32[]{:S(2)}, u32[]{:S(2)}) async-start(bf16[4,16,1024]{2,1,0:T(8,128)(2,1)} %bitcast.6), calls=%async_computation.1 | async-start | bytes 262144 | tf_op jit(solution)/shard_map/all_to_all | solution.py:114
  262.0 27.5 %copy-start.1 = (bf16[1024,1536]{1,0:T(8,128)(2,1)S(1)}, bf16[1024,1536]{1,0:T(8,128)(2,1)}, u32[]{:S(2)}) copy-start(bf16[1024,1536]{1,0:T(8,128)(2,1)} %param.15) | copy-start | bytes 9437188
  (4 other events, 6.1 us)
Sparse Core Ops, SparseCore 0:
  9.6 84.7 all-gather.4
  110.0 21.4 all-gather.8
  133.1 19.6 all-gather.6
  154.2 24.6 all-gather.10
  182.2 68.9 reduce-scatter.1
where the time goes:
time: 297 us; the launch traced here: 296 us
  waiting for transfers between devices  136 us (46%)
  blocking collectives  53.9 us (18%)
  matrix products  31.7 us (11%)
  local copies, waits for them, and re-layouts  31 us (10%)
  other arithmetic  16.2 us (5%)
  between operations  14.1 us (5%)
  starting transfers between devices  13 us (4%)
    all_gather x1, waiting for transfers between devices, per_device(): down_whole = lax.all_gather(w_down, 'tp', axis=1, tiled=True)  72.5 us
    reduce_scatter x1, waiting for transfers between devices, per_device(): lax.psum_scatter(contract_last(select_rows(all_up_act), w_act) + contract...  28.7 us
    unnamed x40, local copies, waits for them, and re-layouts  23.3 us
    all_to_all x1, blocking collectives, per_device(): lax.all_to_all(cotangent, 'tp', split_axis=1, concat_axis=0, tiled=True)  21.8 us
    psum x1, blocking collectives, per_device(): lax.psum((jnp.sum(grad_w_act * grad_w_act, axis=1), jnp.sum(grad_w_val *...  20.2 us
    all_gather x1, waiting for transfers between devices, per_device(): lax.all_gather(grad_up_act, 'tp', axis=0, tiled=True)  18.6 us
    dot_general x3, matrix products, contract_first(): lax.dot_general(left, right, (((0,), (0,)), ((), ())), preferred_element_...  17.5 us
    dot_general x3, matrix products, contract_last(): lax.dot_general(left, right, (((1,), (1,)), ((), ())), preferred_element_...  14.3 us
  transfers between devices with their start and end apart: 10, of which 6 were waited for; matrix products, arithmetic and copies ran while one was open for 21% of the time, Pallas kernels for 0%

commit v1 on v0

v1 whole, which is shorter than its diff:
```python
import functools

import jax
import jax.numpy as jnp
from jax import lax
from jax.experimental import pallas as pl
from jax.experimental.pallas import tpu as pltpu
from jax.sharding import PartitionSpec as P

F32 = jnp.float32
BF16 = jnp.bfloat16
GELU_SCALE = 0.7978845608028654
GELU_CUBIC = 0.044715


def contract(left, right, dims, precision=None):
    return lax.dot_general(
        left, right, ((dims[:1], dims[1:]), ((), ())), precision=precision, preferred_element_type=F32
    )


def tile_of(size, wanted):
    return wanted if size % wanted == 0 else size


def chunk_of(rows):
    return 64 if rows % 64 == 0 else rows


def call(kernel, grid, in_specs, out_specs, out_shape, scratch=(), flops=0):
    return pl.pallas_call(
        kernel,
        grid=grid,
        in_specs=in_specs,
        out_specs=out_specs,
        out_shape=out_shape,
        scratch_shapes=scratch,
        cost_estimate=pl.CostEstimate(flops=flops, transcendentals=0, bytes_accessed=flops // 256),
        compiler_params=pltpu.CompilerParams(
            dimension_semantics=("arbitrary",), vmem_limit_bytes=48 * 1024 * 1024
        ),
    )


def shifted_back(ref, start, rows, reach):
    current = ref[start : start + rows, :].astype(F32)
    if start == 0:
        before = jnp.zeros((8, current.shape[1]), F32)
    else:
        before = ref[start - 16 : start, :].astype(F32)[8:]
    joined = jnp.concatenate([before, current], 0)
    return [joined[8 - reach + k : 8 - reach + k + rows] for k in range(reach)] + [current]


def forward_kernel(up_act, up_val, conv_act, conv_val, bias_act, bias_val, mixed, slope, gate):
    total = up_act.shape[0]
    reach = conv_act.shape[0] - 1
    rows = chunk_of(total)

    def conv(ref, taps, bias, start):
        value = bias[...].astype(F32)
        weights = taps[...].astype(F32)
        for k, shifted in enumerate(shifted_back(ref, start, rows, reach)):
            value = value + weights[k : k + 1] * shifted
        return value

    for start in range(0, total, rows):
        here = slice(start, start + rows)
        act = conv(up_act, conv_act, bias_act, start)
        val = conv(up_val, conv_val, bias_val, start)
        square = act * act
        bent = jnp.tanh(act * (GELU_SCALE + (GELU_SCALE * GELU_CUBIC) * square))
        half = 0.5 + 0.5 * bent
        gelu = act * half
        inner = GELU_SCALE + (3.0 * GELU_SCALE * GELU_CUBIC) * square
        back = half + 0.5 * act * (1.0 - bent * bent) * inner
        mixed[here, :] = (gelu * val).astype(BF16)
        slope[here, :] = back * val
        gate[here, :] = gelu


def backward_kernel(
    core, mine, theirs, slope, gate, up_act, up_val, conv_act, conv_val, w_act, w_val,
    grad_act, grad_val, stats, partial, acc, *, tp_count, fs_count,
):
    total = up_act.shape[0]
    half = total // 2
    reach = conv_act.shape[0] - 1
    rows = chunk_of(half)
    first = core[0] == 0

    def mixed_grad(start, count):
        low = start < half
        at = slice(start % half, start % half + count)
        own, other = mine[at, :], theirs[at, :]
        own, other = own.astype(F32), other.astype(F32)
        return jnp.where(first == low, own, other)

    weights = (conv_act[...].astype(F32), conv_val[...].astype(F32))
    sums = [[None] * (reach + 2), [None] * (reach + 2)]

    def fold(value):
        if rows % 8 == 0:
            return jnp.sum(value.reshape(rows // 8, 8, value.shape[1]), axis=0)
        return jnp.sum(value, axis=0, keepdims=True)

    for start in range(0, total, rows):
        here = slice(start, start + rows)
        grad = mixed_grad(start, rows)
        last = start + rows >= total
        if not last:
            grad_next = mixed_grad(start + rows, 16)[:8]
        for role, (factor, up, out) in enumerate(
            ((slope, up_act, grad_act), (gate, up_val, grad_val))
        ):
            pre = grad * factor[here, :]
            if last:
                after = jnp.zeros((8, pre.shape[1]), F32)
            else:
                after = grad_next * factor[start + rows : start + rows + 8, :]
            joined = jnp.concatenate([pre, after], 0)
            source = up[here, :].astype(F32)
            value = None
            for k in range(reach + 1):
                ahead = reach - k
                moved = joined[ahead : ahead + rows] if ahead else pre
                term = weights[role][k : k + 1] * moved
                value = term if value is None else value + term
                add = fold(moved * source)
                sums[role][k] = add if sums[role][k] is None else sums[role][k] + add
            add = fold(pre)
            sums[role][-1] = add if sums[role][-1] is None else sums[role][-1] + add
            out[here, :] = value.astype(BF16)
    lines = [jnp.sum(entry, axis=0, keepdims=True) for role in sums for entry in role]
    for index, line in enumerate(lines):
        stats[index : index + 1, :] = line

    product = contract(grad_act[...], w_act[...], (1, 1)) + contract(
        grad_val[...], w_val[...], (1, 1)
    )
    step = pl.program_id(0)

    @pl.when(step == 0)
    def _():
        acc[...] = product

    @pl.when(step > 0)
    def _():
        acc[...] += product

    @pl.when(step == pl.num_programs(0) - 1)
    def _():
        shard = total // (tp_count * fs_count)
        for f in range(fs_count):
            for i in range(tp_count):
                start = (i * fs_count + f) * shard
                partial[f, i * shard : (i + 1) * shard, :] = acc[start : start + shard, :].astype(BF16)


def weight_kernel(left, *refs):
    count = len(refs) // 3
    for right, out, squares in zip(refs[:count], refs[count : 2 * count], refs[2 * count :]):
        value = contract(left[...], right[...], (0, 0))
        out[...] = value
        value = value * value
        width = value.shape[1]
        if width % 128 == 0:
            value = functools.reduce(
                jnp.add, [value[:, at : at + 128] for at in range(0, width, 128)]
            )
        ones = jnp.ones((8, value.shape[1]), F32)
        squares[...] = contract(ones, value, (1, 1), lax.Precision.HIGHEST)[:1]


def weight_grads(left, rights):
    rows, height = left.shape
    tile = tile_of(height, 256)
    width = rights[0].shape[1]
    count = len(rights)
    out = call(
        weight_kernel,
        (height // tile,),
        [pl.BlockSpec((rows, tile), lambda i: (0, i))]
        + [pl.BlockSpec((rows, width), lambda i: (0, 0))] * count,
        [pl.BlockSpec((tile, width), lambda i: (i, 0))] * count
        + [pl.BlockSpec((1, tile), lambda i: (0, i))] * count,
        [jax.ShapeDtypeStruct((height, width), F32)] * count
        + [jax.ShapeDtypeStruct((1, height), F32)] * count,
        flops=2 * rows * height * width * count,
    )(left, *rights)
    return out[:count], [entry.reshape(height) for entry in out[count:]]


def per_device(
    hidden_in,
    up_act,
    up_val,
    cotangent,
    w_act,
    w_val,
    w_down,
    conv_act,
    conv_val,
    bias_act,
    bias_val,
):
    local_rows = cotangent.shape[0]
    tap_count = conv_act.shape[0]
    tp_count = lax.axis_size("tp")
    fs_count = lax.axis_size("fs")
    chips = tp_count // 2
    total = local_rows * tp_count
    half = total // 2
    units = up_act.shape[1]
    width = w_act.shape[0]
    core = lax.axis_index("tp") % 2
    swap_cores = [(i, i ^ 1) for i in range(tp_count)]

    all_act = lax.all_gather(up_act, "tp", axis=0, tiled=True)
    all_val = lax.all_gather(up_val, "tp", axis=0, tiled=True)
    cot_blocks = jnp.transpose(cotangent.reshape(local_rows, tp_count, width), (1, 0, 2))
    cot_columns = lax.all_to_all(cot_blocks, "tp", split_axis=0, concat_axis=0, tiled=True)
    cot_columns = cot_columns.reshape(total, width)

    tile = tile_of(units, 256)
    column = pl.BlockSpec((total, tile), lambda i: (0, i))
    taps_spec = pl.BlockSpec((tap_count, tile), lambda i: (0, i))
    line_spec = pl.BlockSpec((1, tile), lambda i: (0, i))
    mixed, slope, gate = call(
        forward_kernel,
        (units // tile,),
        [column, column, taps_spec, taps_spec, line_spec, line_spec],
        [column] * 3,
        [
            jax.ShapeDtypeStruct((total, units), BF16),
            jax.ShapeDtypeStruct((total, units), F32),
            jax.ShapeDtypeStruct((total, units), F32),
        ],
        flops=60 * total * units,
    )(all_act, all_val, conv_act, conv_val, bias_act.reshape(1, units), bias_val.reshape(1, units))

    away = contract(
        lax.dynamic_slice_in_dim(cot_columns, (1 - core) * half, half, 0), w_down, (1, 1)
    ).astype(BF16)
    arrived = lax.ppermute(away, "tp", swap_cores)
    kept = contract(lax.dynamic_slice_in_dim(cot_columns, core * half, half, 0), w_down, (1, 1))
    chip_sum = (kept + arrived.astype(F32)).astype(BF16)
    if chips == 2:
        other = lax.ppermute(chip_sum, "tp", [(i, (i + 2) % tp_count) for i in range(tp_count)])
        mine = (chip_sum.astype(F32) + other.astype(F32)).astype(BF16)
    else:
        groups = [list(range(c, tp_count, 2)) for c in range(2)]
        parts = lax.all_gather(chip_sum, "tp", axis=0, axis_index_groups=groups)
        mine = jnp.sum(parts.astype(F32), axis=0).astype(BF16)
    theirs = lax.ppermute(mine, "tp", swap_cores)

    (grad_w_down,), (down_squares,) = weight_grads(mixed, (cot_columns,))

    shard = local_rows // fs_count
    half_spec = pl.BlockSpec((half, tile), lambda i: (0, i))
    weight_spec = pl.BlockSpec((width, tile), lambda i: (0, i))
    stat_count = 2 * (tap_count + 1)
    grad_act, grad_val, stats, partial = call(
        functools.partial(backward_kernel, tp_count=tp_count, fs_count=fs_count),
        (units // tile,),
        [pl.BlockSpec(memory_space=pltpu.SMEM)]
        + [half_spec] * 2
        + [column] * 4
        + [taps_spec] * 2
        + [weight_spec] * 2,
        [
            column,
            column,
            pl.BlockSpec((stat_count, tile), lambda i: (0, i)),
            pl.BlockSpec((fs_count, tp_count * shard, width), lambda i: (0, 0, 0)),
        ],
        [
            jax.ShapeDtypeStruct((total, units), BF16),
            jax.ShapeDtypeStruct((total, units), BF16),
            jax.ShapeDtypeStruct((stat_count, units), F32),
            jax.ShapeDtypeStruct((fs_count, tp_count * shard, width), BF16),
        ],
        scratch=[pltpu.VMEM((total, width), F32)],
        flops=4 * total * units * width,
    )(
        core.reshape(1).astype(jnp.int32),
        mine,
        theirs,
        slope,
        gate,
        all_act,
        all_val,
        conv_act,
        conv_val,
        w_act,
        w_val,
    )
    pieces = lax.all_to_all(partial, "fs", split_axis=0, concat_axis=0, tiled=True)
    (grad_w_act, grad_w_val), (act_squares, val_squares) = weight_grads(
        hidden_in, (grad_act, grad_val)
    )
    taps_act, sums_act = stats[:tap_count], stats[tap_count]
    taps_val, sums_val = stats[tap_count + 1 : 2 * tap_count + 1], stats[2 * tap_count + 1]
    tap_squares = jnp.stack(
        [jnp.sum(taps_act * taps_act, axis=1), jnp.sum(taps_val * taps_val, axis=1)], 0
    )
    rows_down = lax.psum(down_squares, "tp")
    rows_act, rows_val, conv_rows = lax.psum((act_squares, val_squares, tap_squares), "fs")
    summed = jnp.sum(pieces.astype(F32), axis=0).astype(BF16).reshape(tp_count, shard, width)
    blocks = lax.all_to_all(summed, "tp", split_axis=0, concat_axis=0, tiled=True)
    grad_input = jnp.transpose(blocks, (1, 0, 2)).reshape(shard, tp_count * width)
    return (
        grad_input,
        grad_w_act,
        grad_w_val,
        grad_w_down,
        taps_act,
        taps_val,
        sums_act,
        sums_val,
        rows_act,
        rows_val,
        rows_down,
        conv_rows,
    )


def solution(mesh):
    return jax.shard_map(
        per_device,
        mesh=mesh,
        in_specs=(
            P(None, "tp"),
            P("tp", "fs"),
            P("tp", "fs"),
            P("tp", None),
            P("tp", "fs"),
            P("tp", "fs"),
            P("fs", "tp"),
            P(None, "fs"),
            P(None, "fs"),
            P("fs"),
            P("fs"),
        ),
        out_specs=(
            P(("tp", "fs"), None),
            P("tp", "fs"),
            P("tp", "fs"),
            P("fs", "tp"),
            P(None, "fs"),
            P(None, "fs"),
            P("fs"),
            P("fs"),
            P("tp"),
            P("tp"),
            P("fs"),
            P(),
        ),
        check_vma=False,
    )
```

time: 297 us -> 177 us (0.60)
  waiting for transfers between devices: 136 us -> 58.7 us
  Pallas kernels: 0 us -> 34 us
  matrix products: 31.7 us -> 5.25 us
  blocking collectives: 53.9 us -> 29.6 us
  local copies, waits for them, and re-layouts: 31 us -> 16.5 us
  other arithmetic: 16.2 us -> 3.96 us
    all_gather x4 -> x2, waiting for transfers between devices: 101 us -> 0.04 us  [the longest x1 0.02 us: per_device(): all_act = lax.all_gather(up_act, 'tp', axis=0, tiled=True)]
    pallas_call x0 -> x4, Pallas kernels: none -> 34 us  [the longest x2 14.1 us: weight_grads(): call(weight_kernel, (height // tile,), [pl.BlockSpec((rows, tile), lambda...]
    reduce_scatter x1 -> x0, waiting for transfers between devices: 28.7 us -> none  [per_device(): lax.psum_scatter(contract_last(select_rows(all_up_act), w_act) + contract...]
    all_to_all x1 -> x3, waiting for transfers between devices: 0.01 us -> 27.5 us  [the longest x1 23.5 us: per_device(): lax.all_to_all(cot_blocks, 'tp', split_axis=0, concat_axis=0, tiled=True)]
    dot_general x6 -> x2, matrix products: 31.7 us -> 5.25 us  [contract(): lax.dot_general(left, right, ((dims[:1], dims[1:]), ((), ())), precision=...]
    ppermute x4 -> x3, waiting for transfers between devices: 5.15 us -> 30.5 us  [the longest x1 28 us: per_device(): lax.ppermute(chip_sum, 'tp', [(i, (i + 2) % tp_count) for i in range(tp_c...]
    all_to_all x1 -> x0, blocking collectives: 21.8 us -> none  [per_device(): lax.all_to_all(cotangent, 'tp', split_axis=1, concat_axis=0, tiled=True)]
    all_to_all x1 -> x3, starting transfers between devices: 3.33 us -> 14.2 us  [the longest x1 6.64 us: per_device(): lax.all_to_all(partial, 'fs', split_axis=0, concat_axis=0, tiled=True)]
  transfers between devices with their start and end apart: 10 -> 8, of which waited for: 6 -> 4; matrix products, arithmetic and copies ran while one was open for 21% -> 6% of each run, Pallas kernels for 0% -> 12%
where the time goes in v1:
time: 177 us
  waiting for transfers between devices  58.7 us (33%)
  Pallas kernels  34 us (19%)
  blocking collectives  29.6 us (17%)
  local copies, waits for them, and re-layouts  16.5 us (9%)
  starting transfers between devices  14.4 us (8%)
  between operations  14.3 us (8%)
  matrix products  5.25 us (3%)
  other arithmetic  3.96 us (2%)
    ppermute x1, waiting for transfers between devices, per_device(): lax.ppermute(chip_sum, 'tp', [(i, (i + 2) % tp_count) for i in range(tp_c...  28 us
    all_to_all x1, waiting for transfers between devices, per_device(): lax.all_to_all(cot_blocks, 'tp', split_axis=0, concat_axis=0, tiled=True)  23.5 us
    psum x1, blocking collectives, per_device(): lax.psum((act_squares, val_squares, tap_squares), 'fs')  22.7 us
    pallas_call x2, Pallas kernels, weight_grads(): call(weight_kernel, (height // tile,), [pl.BlockSpec((rows, tile), lambda...  14.1 us
    pallas_call x1, Pallas kernels, per_device(): call(functools.partial(backward_kernel, tp_count=tp_count, fs_count=fs_co...  12.7 us
    unnamed x30, local copies, waits for them, and re-layouts  12.7 us
    pallas_call x1, Pallas kernels, per_device(): call(forward_kernel, (units // tile,), [column, column, taps_spec, taps_s...  7.14 us
    psum x1, blocking collectives, per_device(): rows_down = lax.psum(down_squares, 'tp')  6.95 us
  transfers between devices with their start and end apart: 8, of which 4 were waited for; matrix products, arithmetic and copies ran while one was open for 6% of the time, Pallas kernels for 12%

profile of v1, /device:TPU:0, one launch (start us, length us, event | category | flops | bytes accessed | tf_op | source)
XLA Modules:
  0.0 176.7 jit_solution(12239204573031668231)
XLA Ops:
  7.9 2.5 %copy.30 = bf16[16,4,8,1024]{3,2,0,1:T(8,128)(2,1)} copy(bf16[16,4,8,1024]{3,2,1,0:T(8,128)(2,1)} %bitcast.22) | data formatting | bytes 2097152 | tf_op jit(solution)/shard_map/reshape | solution.py:221
  10.4 4.3 %all-to-all-start = ((bf16[4,128,1024]{2,1,0:T(8,128)(2,1)}), bf16[4,128,1024]{2,1,0:T(8,128)(2,1)}, u32[]{:S(2)}, u32[]{:S(2)}) async-start(bf16[4,128,1024]{2,1,0:T(8,128)(2,1)} %bitcast.21), calls=%async_computation | async-start | bytes 2097152 | tf_op jit(solution)/shard_map/all_to_all | solution.py:222
  14.7 23.5 %all-to-all-done = bf16[4,128,1024]{2,1,0:T(8,128)(2,1)} async-done(((bf16[4,128,1024]{2,1,0:T(8,128)(2,1)}), bf16[4,128,1024]{2,1,0:T(8,128)(2,1)}, u32[]{:S(2)}, u32[]{:S(2)}) %all-to-all-start) | async-done | bytes 1048608 | tf_op jit(solution)/shard_map/all_to_all | solution.py:222
  38.3 2.9 %convolution_convert_fusion = bf16[256,1536]{1,0:T(8,128)(2,1)} fusion(bf16[1536,1024]{1,0:T(8,128)(2,1)S(1)} %copy-done, bf16[512,1024]{1,0:T(8,128)(2,1)} %bitcast.2.refs_0_, s32[]{:T(128)S(6)} %select_n.15), kind=kOutput, calls=%fused_computation | convolution fusion | flops 805699584 | bytes 4456452 | tf_op jit(solution)/shard_map/dot_general | solution.py:17
  41.3 2.5 %collective-permute-done = bf16[256,1536]{1,0:T(8,128)(2,1)} collective-permute-done((bf16[256,1536]{1,0:T(8,128)(2,1)}, bf16[256,1536]{1,0:T(8,128)(2,1)}, u32[]{:S(2)}, u32[]{:S(2)}) %collective-permute-start) | collective-permute-done | bytes 786464 | tf_op jit(solution)/shard_map/ppermute | solution.py:245
  43.8 2.3 %add_convert_fusion.1 = bf16[256,1536]{1,0:T(8,128)(2,1)S(1)} fusion(bf16[256,1536]{1,0:T(8,128)(2,1)} %collective-permute-done, bf16[1536,1024]{1,0:T(8,128)(2,1)S(1)} %copy-done, bf16[512,1024]{1,0:T(8,128)(2,1)} %bitcast.2.refs_0_, s32[]{:T(128)S(6)} %select_n.14), kind=kOutput, calls=%fused_computation.2 | convolution fusion | flops 806486016 | bytes 5242884 | tf_op jit(solution)/shard_map/dot_general | solution.py:17
  46.2 28.0 %collective-permute-done.1 = bf16[256,1536]{1,0:T(8,128)(2,1)S(1)} collective-permute-done((bf16[256,1536]{1,0:T(8,128)(2,1)S(1)}, bf16[256,1536]{1,0:T(8,128)(2,1)S(1)}, u32[]{:S(2)}, u32[]{:S(2)}) %collective-permute-start.1) | collective-permute-done | bytes 786464 | tf_op jit(solution)/shard_map/ppermute | solution.py:249
  75.4 1.4 copy-done.1
  76.8 1.4 copy-done.2
  78.2 7.1 %shard_map.202 = (bf16[512,1536]{1,0:T(8,128)(2,1)S(1)}, f32[512,1536]{1,0:T(8,128)}, f32[512,1536]{1,0:T(8,128)}) custom-call(bf16[512,1536]{1,0:T(8,128)(2,1)S(1)} %copy-done.1, bf16[512,1536]{1,0:T(8,128)(2,1)S(1)} %copy-done.2, bf16[3,1536]{1,0:T(4,128)(2,1)S(1)} %copy-done.4, bf16[3,1536]{1,0:T(4,128)(2,1)S(1)} %copy-done.5, ...), custom_call_target="tpu_custom_call" | custom-call | flops 47185920 | bytes 184320 | tf_op jit(solution)/shard_map/pallas_call | solution.py:229
  85.4 1.1 copy-done.10
  86.5 12.7 %shard_map.203 = (bf16[512,1536]{1,0:T(8,128)(2,1)S(1)}, bf16[512,1536]{1,0:T(8,128)(2,1)S(1)}, f32[8,1536]{1,0:T(8,128)S(1)}, bf16[8,64,1024]{2,1,0:T(8,128)(2,1)S(1)}) custom-call(s32[1]{0:T(128)} %bitcast.core, bf16[256,1536]{1,0:T(8,128)(2,1)} %add_convert_fusion.mine, bf16[256,1536]{1,0:T(8,128)(2,1)} %collective-permute-done.2.theirs, ...), custom_call_target="tpu_custom_call" | custom-call | flops 3221225472 | bytes 12582912 | tf_op jit(solution)/shard_map/pallas_call | solution.py:263
  102.5 6.6 %all-to-all-start.1 = ((bf16[8,64,1024]{2,1,0:T(8,128)(2,1)}), bf16[8,64,1024]{2,1,0:T(8,128)(2,1)}, u32[]{:S(2)}, u32[]{:S(2)}) async-start(bf16[8,64,1024]{2,1,0:T(8,128)(2,1)} %copy-done.3), calls=%async_computation.1 | async-start | bytes 2097152 | tf_op jit(solution)/shard_map/all_to_all | solution.py:298
  109.2 1.4 copy-done.11
  110.6 6.8 %shard_map.205 = (f32[1536,1024]{1,0:T(8,128)}, f32[1,1536]{1,0:T(1,128)S(1)}) custom-call(bf16[512,1536]{1,0:T(8,128)(2,1)S(1)} %copy-done.11, bf16[512,1024]{1,0:T(8,128)(2,1)} %bitcast.2.refs_0_), custom_call_target="tpu_custom_call" | custom-call | flops 1610612736 | bytes 6291456 | tf_op jit(solution)/shard_map/pallas_call | solution.py:180
  117.4 7.0 %psum.30 = f32[1536]{0:T(1024)} all-reduce(f32[1536]{0:T(1024)S(1)} %reduce.3), channel_id=1, replica_groups=mesh['fs'=8,'tp'=4] {'tp'}, use_global_device_ids=true, to_apply=%region_3.4 | all-reduce | flops 1536 | bytes 12288 | tf_op jit(solution)/shard_map/psum | solution.py:307
  125.2 1.4 copy-done.7
  126.6 1.4 copy-done.9
  128.0 1.2 copy-done.12
  129.2 7.3 %shard_map.204 = (f32[1024,1536]{1,0:T(8,128)}, f32[1024,1536]{1,0:T(8,128)}, f32[1,1024]{1,0:T(1,128)S(1)}, f32[1,1024]{1,0:T(1,128)S(1)}) custom-call(bf16[512,1024]{1,0:T(8,128)(2,1)S(1)} %copy-done.12, bf16[512,1536]{1,0:T(8,128)(2,1)S(1)} %copy-done.7, bf16[512,1536]{1,0:T(8,128)(2,1)S(1)} %copy-done.9), custom_call_target="tpu_custom_call" | custom-call | flops 3221225472 | bytes 12582912 | tf_op jit(solution)/shard_map/pallas_call | solution.py:180
  136.5 22.7 %all-reduce = (f32[1024]{0:T(1024)}, f32[1024]{0:T(1024)}, f32[2,3]{1,0:T(2,128)}) all-reduce(f32[1024]{0:T(1024)S(1)} %bitcast.19, f32[1024]{0:T(1024)S(1)} %bitcast.20, f32[2,3]{1,0:T(2,128)S(1)} %pad_maximum_fusion), channel_id=1, replica_groups=mesh['fs'=8,'tp'=4] {'fs'}, use_global_device_ids=true, to_apply=%region_1.2 | all-reduce | flops 2054 | bytes 16432 | tf_op jit(solution)/shard_map/psum | solution.py:308
  159.2 2.1 %reduce_sum.30 = bf16[64,1024]{1,0:T(8,128)(2,1)} reduce(bf16[8,64,1024]{2,1,0:T(8,128)(2,1)} %all-to-all-done.1, bf16[]{:T(256)} %constant.25.clone.1), dimensions={0}, to_apply=%region_0.1 | reduce | flops 458752 | bytes 1179650 | tf_op jit(solution)/shard_map/reduce_sum | solution.py:309
  161.3 3.3 %all-to-all-start.2 = ((bf16[4,16,1024]{2,1,0:T(8,128)(2,1)}), bf16[4,16,1024]{2,1,0:T(8,128)(2,1)S(1)}, u32[]{:S(2)}, u32[]{:S(2)}) async-start(bf16[4,16,1024]{2,1,0:T(8,128)(2,1)} %bitcast.3), calls=%async_computation.2 | async-start | bytes 262144 | tf_op jit(solution)/shard_map/all_to_all | solution.py:310
  165.2 3.9 %all-to-all-done.2 = bf16[4,16,1024]{2,1,0:T(8,128)(2,1)S(1)} async-done(((bf16[4,16,1024]{2,1,0:T(8,128)(2,1)}), bf16[4,16,1024]{2,1,0:T(8,128)(2,1)S(1)}, u32[]{:S(2)}, u32[]{:S(2)}) %all-to-all-start.2) | async-done | bytes 131104 | tf_op jit(solution)/shard_map/all_to_all | solution.py:310
  (42 shorter events, 7.4 us)
Async XLA Ops:
  7.2 31.1 %copy-start = (bf16[1536,1024]{1,0:T(8,128)(2,1)S(1)}, bf16[1536,1024]{1,0:T(8,128)(2,1)}, u32[]{:S(2)}) copy-start(bf16[1536,1024]{1,0:T(8,128)(2,1)} %param.17) | copy-start | bytes 9437188
  7.2 68.2 %all-gather.3.cloned.1.call-start = ((), (), s32[]{:S(2)}) async-start(), calls=%async_computation.3 | async-start | bytes 1966080 | tf_op jit(solution)/shard_map/all_gather | solution.py:219
  10.4 27.8 %all-to-all-start = ((bf16[4,128,1024]{2,1,0:T(8,128)(2,1)}), bf16[4,128,1024]{2,1,0:T(8,128)(2,1)}, u32[]{:S(2)}, u32[]{:S(2)}) async-start(bf16[4,128,1024]{2,1,0:T(8,128)(2,1)} %bitcast.21), calls=%async_computation | async-start | bytes 2097152 | tf_op jit(solution)/shard_map/all_to_all | solution.py:222
  14.7 60.7 %all-gather.5.cloned.1.call-start = ((), (), s32[]{:S(2)}) async-start(), calls=%async_computation.4 | async-start | bytes 1966080 | tf_op jit(solution)/shard_map/all_gather | solution.py:220
  41.2 2.6 %collective-permute-start = (bf16[256,1536]{1,0:T(8,128)(2,1)}, bf16[256,1536]{1,0:T(8,128)(2,1)}, u32[]{:S(2)}, u32[]{:S(2)}) collective-permute-start(bf16[256,1536]{1,0:T(8,128)(2,1)} %convolution_convert_fusion), channel_id=1, source_target_pairs={{0,1},{1,0},{2,3},{3,2},{4,5},{5,4},{6,7},{7,6},{8,9},{9,8},{10,11... | collective-permute-start | bytes 2359304 | tf_op jit(solution)/shard_map/ppermute | solution.py:245
  41.2 34.1 %copy-start.13 = (bf16[1536]{0:T(1024)(128)(2,1)S(1)}, bf16[1536]{0:T(1024)(128)(2,1)}, u32[]{:S(2)}) copy-start(bf16[1536]{0:T(1024)(128)(2,1)} %param.20) | copy-start | bytes 9220
  41.2 34.1 %copy-start.14 = (bf16[1536]{0:T(1024)(128)(2,1)S(1)}, bf16[1536]{0:T(1024)(128)(2,1)}, u32[]{:S(2)}) copy-start(bf16[1536]{0:T(1024)(128)(2,1)} %param.21) | copy-start | bytes 9220
  41.3 34.1 %copy-start.4 = (bf16[3,1536]{1,0:T(4,128)(2,1)S(1)}, bf16[3,1536]{1,0:T(4,128)(2,1)}, u32[]{:S(2)}) copy-start(bf16[3,1536]{1,0:T(4,128)(2,1)} %conv_act.3) | copy-start | bytes 27652
  41.3 34.1 %copy-start.5 = (bf16[3,1536]{1,0:T(4,128)(2,1)S(1)}, bf16[3,1536]{1,0:T(4,128)(2,1)}, u32[]{:S(2)}) copy-start(bf16[3,1536]{1,0:T(4,128)(2,1)} %conv_val.3) | copy-start | bytes 27652
  46.1 28.1 %collective-permute-start.1 = (bf16[256,1536]{1,0:T(8,128)(2,1)S(1)}, bf16[256,1536]{1,0:T(8,128)(2,1)S(1)}, u32[]{:S(2)}, u32[]{:S(2)}) collective-permute-start(bf16[256,1536]{1,0:T(8,128)(2,1)S(1)} %add_convert_fusion.1), channel_id=1, source_target_pairs={{0,2},{1,3},{2,0},{3,1},{4,6},{5,7},{6,4},{7,5},{8,10},{9,11},{10,... | collective-permute-start | bytes 2359304 | tf_op jit(solution)/shard_map/ppermute | solution.py:249
  75.3 11.2 %collective-permute-start.2 = (bf16[256,1536]{1,0:T(8,128)(2,1)}, bf16[256,1536]{1,0:T(8,128)(2,1)}, u32[]{:S(2)}, u32[]{:S(2)}) collective-permute-start(bf16[256,1536]{1,0:T(8,128)(2,1)} %add_convert_fusion.mine), channel_id=1, source_target_pairs={{0,1},{1,0},{2,3},{3,2},{4,5},{5,4},{6,7},{7,6},{8,9},{9,8},{10,11... | collective-permute-start | bytes 2359304 | tf_op jit(solution)/shard_map/ppermute | solution.py:255
  75.4 1.4 copy-start.1
  76.8 1.4 copy-start.2
  85.4 1.1 copy-start.10
  99.3 1.0 copy-start.3
  100.3 1.1 copy-start.6
  101.4 1.1 copy-start.8
  102.5 56.6 %all-to-all-start.1 = ((bf16[8,64,1024]{2,1,0:T(8,128)(2,1)}), bf16[8,64,1024]{2,1,0:T(8,128)(2,1)}, u32[]{:S(2)}, u32[]{:S(2)}) async-start(bf16[8,64,1024]{2,1,0:T(8,128)(2,1)} %copy-done.3), calls=%async_computation.1 | async-start | bytes 2097152 | tf_op jit(solution)/shard_map/all_to_all | solution.py:298
  109.2 1.4 copy-start.11
  125.2 1.4 copy-start.7
  126.6 1.4 copy-start.9
  128.0 1.2 copy-start.12
  161.3 7.9 %all-to-all-start.2 = ((bf16[4,16,1024]{2,1,0:T(8,128)(2,1)}), bf16[4,16,1024]{2,1,0:T(8,128)(2,1)S(1)}, u32[]{:S(2)}, u32[]{:S(2)}) async-start(bf16[4,16,1024]{2,1,0:T(8,128)(2,1)} %bitcast.3), calls=%async_computation.2 | async-start | bytes 262144 | tf_op jit(solution)/shard_map/all_to_all | solution.py:310
Sparse Core Ops, SparseCore 0:
  9.6 30.0 all-gather.2
  41.3 29.4 all-gather.4

commit v2 on v1

--- a/solution.py
+++ b/solution.py
@@ -11,6 +11,8 @@
 BF16 = jnp.bfloat16
 GELU_SCALE = 0.7978845608028654
 GELU_CUBIC = 0.044715
+COT_OVER_FS = False
+TIED = True
 
 
 def contract(left, right, dims, precision=None):
@@ -25,6 +27,16 @@
 
 def chunk_of(rows):
     return 64 if rows % 64 == 0 else rows
+
+
+def in_hbm(value):
+    return pltpu.with_memory_space_constraint(value, pltpu.HBM)
+
+
+def copies_over(vector, axis):
+    count = lax.axis_size(axis)
+    spread = jnp.broadcast_to(vector[None], (count,) + vector.shape)
+    return jnp.sum(lax.all_to_all(spread, axis, split_axis=0, concat_axis=0, tiled=True), axis=0)
 
 
 def call(kernel, grid, in_specs, out_specs, out_shape, scratch=(), flops=0):
@@ -52,7 +64,13 @@
     return [joined[8 - reach + k : 8 - reach + k + rows] for k in range(reach)] + [current]
 
 
-def forward_kernel(up_act, up_val, conv_act, conv_val, bias_act, bias_val, mixed, slope, gate):
+def forward_kernel(places, *refs, pieces):
+    conv_act, conv_val, bias_act, bias_val, mixed, slope, gate, up_act, up_val = refs[2 * pieces :]
+    for index in range(pieces):
+        count = refs[index].shape[0]
+        start = pl.multiple_of(places[index] * count, count)
+        up_act[pl.ds(start, count), :] = refs[index][...]
+        up_val[pl.ds(start, count), :] = refs[pieces + index][...]
     total = up_act.shape[0]
     reach = conv_act.shape[0] - 1
     rows = chunk_of(total)
@@ -184,10 +202,10 @@
         + [pl.BlockSpec((rows, width), lambda i: (0, 0))] * count,
         [pl.BlockSpec((tile, width), lambda i: (i, 0))] * count
         + [pl.BlockSpec((1, tile), lambda i: (0, i))] * count,
-        [jax.ShapeDtypeStruct((height, width), F32)] * count
+        [pltpu.HBM((height, width), F32)] * count
         + [jax.ShapeDtypeStruct((1, height), F32)] * count,
         flops=2 * rows * height * width * count,
-    )(left, *rights)
+    )(in_hbm(left), *[in_hbm(right) for right in rights])
     return out[:count], [entry.reshape(height) for entry in out[count:]]
 
 
@@ -216,28 +234,55 @@
     core = lax.axis_index("tp") % 2
     swap_cores = [(i, i ^ 1) for i in range(tp_count)]
 
-    all_act = lax.all_gather(up_act, "tp", axis=0, tiled=True)
-    all_val = lax.all_gather(up_val, "tp", axis=0, tiled=True)
-    cot_blocks = jnp.transpose(cotangent.reshape(local_rows, tp_count, width), (1, 0, 2))
-    cot_columns = lax.all_to_all(cot_blocks, "tp", split_axis=0, concat_axis=0, tiled=True)
-    cot_columns = cot_columns.reshape(total, width)
+    shard = local_rows // fs_count
+    if COT_OVER_FS:
+        own_rows = lax.dynamic_slice_in_dim(cotangent, lax.axis_index("fs") * shard, shard, 0)
+        own_rows = jnp.transpose(own_rows.reshape(shard, tp_count, width), (1, 0, 2))
+        own_rows = lax.all_to_all(own_rows, "tp", split_axis=0, concat_axis=0, tiled=True)
+        cot_columns = lax.all_gather(own_rows, "fs", axis=0)
+        cot_columns = jnp.transpose(cot_columns, (1, 0, 2, 3)).reshape(total, width)
+    else:
+        cot_blocks = jnp.transpose(cotangent.reshape(local_rows, tp_count, width), (1, 0, 2))
+        cot_columns = lax.all_to_all(cot_blocks, "tp", split_axis=0, concat_axis=0, tiled=True)
+        cot_columns = cot_columns.reshape(total, width)
+        if TIED:
+            cot_columns, up_act, up_val = lax.optimization_barrier((cot_columns, up_act, up_val))
+    place = lax.axis_index("tp").astype(jnp.int32)
+    if chips == 2:
+        swap_chips = [(i, (i + 2) % tp_count) for i in range(tp_count)]
+        ups = (up_act, up_val)
+        across = [lax.ppermute(entry, "tp", swap_chips) for entry in ups]
+        beside = [lax.ppermute(entry, "tp", swap_cores) for entry in ups]
+        corner = [lax.ppermute(entry, "tp", swap_cores) for entry in across]
+        gathered = [[ups[r], beside[r], across[r], corner[r]] for r in range(2)]
+        places = jnp.stack([place, place ^ 1, place ^ 2, place ^ 3])
+    else:
+        gathered = [[lax.all_gather(entry, "tp", axis=0, tiled=True)] for entry in (up_act, up_val)]
+        places = jnp.zeros((1,), jnp.int32)
+    pieces = len(gathered[0])
 
     tile = tile_of(units, 256)
     column = pl.BlockSpec((total, tile), lambda i: (0, i))
     taps_spec = pl.BlockSpec((tap_count, tile), lambda i: (0, i))
     line_spec = pl.BlockSpec((1, tile), lambda i: (0, i))
-    mixed, slope, gate = call(
-        forward_kernel,
+    piece = pl.BlockSpec((total // pieces, tile), lambda i: (0, i))
+    mixed, slope, gate, all_act, all_val = call(
+        functools.partial(forward_kernel, pieces=pieces),
         (units // tile,),
-        [column, column, taps_spec, taps_spec, line_spec, line_spec],
-        [column] * 3,
-        [
-            jax.ShapeDtypeStruct((total, units), BF16),
-            jax.ShapeDtypeStruct((total, units), F32),
-            jax.ShapeDtypeStruct((total, units), F32),
-        ],
+        [pl.BlockSpec(memory_space=pltpu.SMEM)]
+        + [piece] * (2 * pieces)
+        + [taps_spec, taps_spec, line_spec, line_spec],
+        [column] * 5,
+        [pltpu.HBM((total, units), dtype) for dtype in (BF16, F32, F32, BF16, BF16)],
         flops=60 * total * units,
-    )(all_act, all_val, conv_act, conv_val, bias_act.reshape(1, units), bias_val.reshape(1, units))
+    )(
+        places,
+        *[in_hbm(entry) for entry in gathered[0] + gathered[1]],
+        conv_act,
+        conv_val,
+        bias_act.reshape(1, units),
+        bias_val.reshape(1, units),
+    )
 
     away = contract(
         lax.dynamic_slice_in_dim(cot_columns, (1 - core) * half, half, 0), w_down, (1, 1)
@@ -246,7 +291,7 @@
     kept = contract(lax.dynamic_slice_in_dim(cot_columns, core * half, half, 0), w_down, (1, 1))
     chip_sum = (kept + arrived.astype(F32)).astype(BF16)
     if chips == 2:
-        other = lax.ppermute(chip_sum, "tp", [(i, (i + 2) % tp_count) for i in range(tp_count)])
+        other = lax.ppermute(chip_sum, "tp", swap_chips)
         mine = (chip_sum.astype(F32) + other.astype(F32)).astype(BF16)
     else:
         groups = [list(range(c, tp_count, 2)) for c in range(2)]
@@ -256,7 +301,6 @@
 
     (grad_w_down,), (down_squares,) = weight_grads(mixed, (cot_columns,))
 
-    shard = local_rows // fs_count
     half_spec = pl.BlockSpec((half, tile), lambda i: (0, i))
     weight_spec = pl.BlockSpec((width, tile), lambda i: (0, i))
     stat_count = 2 * (tap_count + 1)
@@ -275,27 +319,27 @@
             pl.BlockSpec((fs_count, tp_count * shard, width), lambda i: (0, 0, 0)),
         ],
         [
-            jax.ShapeDtypeStruct((total, units), BF16),
-            jax.ShapeDtypeStruct((total, units), BF16),
+            pltpu.HBM((total, units), BF16),
+            pltpu.HBM((total, units), BF16),
             jax.ShapeDtypeStruct((stat_count, units), F32),
-            jax.ShapeDtypeStruct((fs_count, tp_count * shard, width), BF16),
+            pltpu.HBM((fs_count, tp_count * shard, width), BF16),
         ],
         scratch=[pltpu.VMEM((total, width), F32)],
         flops=4 * total * units * width,
     )(
         core.reshape(1).astype(jnp.int32),
-        mine,
-        theirs,
-        slope,
-        gate,
-        all_act,
-        all_val,
+        in_hbm(mine),
+        in_hbm(theirs),
+        in_hbm(slope),
+        in_hbm(gate),
+        in_hbm(all_act),
+        in_hbm(all_val),
         conv_act,
         conv_val,
-        w_act,
-        w_val,
-    )
-    pieces = lax.all_to_all(partial, "fs", split_axis=0, concat_axis=0, tiled=True)
+        in_hbm(w_act),
+        in_hbm(w_val),
+    )
+    terms = lax.all_to_all(partial, "fs", split_axis=0, concat_axis=0, tiled=True)
     (grad_w_act, grad_w_val), (act_squares, val_squares) = weight_grads(
         hidden_in, (grad_act, grad_val)
     )
@@ -304,9 +348,12 @@
     tap_squares = jnp.stack(
         [jnp.sum(taps_act * taps_act, axis=1), jnp.sum(taps_val * taps_val, axis=1)], 0
     )
-    rows_down = lax.psum(down_squares, "tp")
-    rows_act, rows_val, conv_rows = lax.psum((act_squares, val_squares, tap_squares), "fs")
-    summed = jnp.sum(pieces.astype(F32), axis=0).astype(BF16).reshape(tp_count, shard, width)
+    rows_down = copies_over(down_squares, "tp")
+    lines = jnp.concatenate([act_squares, val_squares, tap_squares.reshape(-1)])
+    lines = copies_over(lines, "fs")
+    rows_act, rows_val = lines[:width], lines[width : 2 * width]
+    conv_rows = lines[2 * width :].reshape(tap_squares.shape)
+    summed = jnp.sum(terms.astype(F32), axis=0).astype(BF16).reshape(tp_count, shard, width)
     blocks = lax.all_to_all(summed, "tp", split_axis=0, concat_axis=0, tiled=True)
     grad_input = jnp.transpose(blocks, (1, 0, 2)).reshape(shard, tp_count * width)
     return (

time: 177 us -> 169 us (0.955)
  waiting for transfers between devices: 58.7 us -> 79.9 us
  blocking collectives: 29.6 us -> 13.4 us
  between operations: 14.3 us -> 0.82 us
  local copies, waits for them, and re-layouts: 16.5 us -> 5.76 us
  Pallas kernels: 34 us -> 39.7 us
  starting transfers between devices: 14.4 us -> 17.8 us
    psum x2 -> x0, blocking collectives: 29.6 us -> none  [the longest x1 22.7 us: per_device(): lax.psum((act_squares, val_squares, tap_squares), 'fs')]
    all_to_all x1, waiting for transfers between devices: 0.01 us -> 24.1 us  [per_device(): lax.all_to_all(partial, 'fs', split_axis=0, concat_axis=0, tiled=True)]
    all_to_all x0 -> x1, blocking collectives: none -> 13.4 us  [copies_over(): lax.all_to_all(spread, axis, split_axis=0, concat_axis=0, tiled=True)]
    unnamed x30 -> x10, local copies, waits for them, and re-layouts: 12.7 us -> 0.03 us
    all_to_all x1, waiting for transfers between devices: 23.5 us -> 15.1 us  [per_device(): lax.all_to_all(cot_blocks, 'tp', split_axis=0, concat_axis=0, tiled=True)]
    ppermute x1 -> x7, waiting for transfers between devices: 28 us -> 34.8 us  [the longest x1 18.3 us: per_device(): other = lax.ppermute(chip_sum, 'tp', swap_chips)]
    all_to_all x0 -> x1, starting transfers between devices: none -> 3.26 us  [copies_over(): lax.all_to_all(spread, axis, split_axis=0, concat_axis=0, tiled=True)]
    ppermute x1 -> x7, starting transfers between devices: 0.07 us -> 2.68 us  [the longest x2 2.09 us: per_device(): across = [lax.ppermute(entry, 'tp', swap_chips) for entry in ups]]
  transfers between devices with their start and end apart: 8 -> 13, of which waited for: 4 -> 8; matrix products, arithmetic and copies ran while one was open for 6% -> 3% of each run, Pallas kernels for 12% -> 24%
where the time goes in v2:
time: 169 us; the launch traced here: 167 us
  waiting for transfers between devices  79.9 us (47%)
  Pallas kernels  39.7 us (23%)
  starting transfers between devices  17.8 us (11%)
  blocking collectives  13.4 us (8%)
  local copies, waits for them, and re-layouts  5.76 us (3%)
  matrix products  5.24 us (3%)
  other arithmetic  4.74 us (3%)
    all_to_all x1, waiting for transfers between devices, per_device(): lax.all_to_all(partial, 'fs', split_axis=0, concat_axis=0, tiled=True)  24.1 us
    ppermute x1, waiting for transfers between devices, per_device(): other = lax.ppermute(chip_sum, 'tp', swap_chips)  18.3 us
    pallas_call x2, Pallas kernels, weight_grads(): call(weight_kernel, (height // tile,), [pl.BlockSpec((rows, tile), lambda...  16.5 us
    all_to_all x1, waiting for transfers between devices, per_device(): lax.all_to_all(cot_blocks, 'tp', split_axis=0, concat_axis=0, tiled=True)  15.1 us
    ppermute x2, waiting for transfers between devices, per_device(): across = [lax.ppermute(entry, 'tp', swap_chips) for entry in ups]  14.5 us
    pallas_call x1, Pallas kernels, per_device(): call(functools.partial(backward_kernel, tp_count=tp_count, fs_count=fs_co...  14.1 us
    all_to_all x1, blocking collectives, copies_over(): lax.all_to_all(spread, axis, split_axis=0, concat_axis=0, tiled=True)  13.4 us
    pallas_call x1, Pallas kernels, per_device(): call(functools.partial(forward_kernel, pieces=pieces), (units // tile,),...  9.08 us
  transfers between devices with their start and end apart: 13, of which 8 were waited for; matrix products, arithmetic and copies ran while one was open for 3% of the time, Pallas kernels for 24%

profile of v2, /device:TPU:0, one launch (start us, length us, event | category | flops | bytes accessed | tf_op | source)
XLA Modules:
  0.0 167.3 jit_solution(8851427413479404082)
XLA Ops:
  0.7 2.4 %copy.41 = bf16[16,4,8,1024]{3,2,0,1:T(8,128)(2,1)} copy(bf16[16,4,8,1024]{3,2,1,0:T(8,128)(2,1)} %bitcast.26) | data formatting | bytes 2097152 | tf_op jit(solution)/shard_map/reshape | solution.py:245
  3.1 4.3 %all-to-all-start = ((bf16[4,128,1024]{2,1,0:T(8,128)(2,1)}), bf16[4,128,1024]{2,1,0:T(8,128)(2,1)}, u32[]{:S(2)}, u32[]{:S(2)}) async-start(bf16[4,128,1024]{2,1,0:T(8,128)(2,1)} %bitcast.25), calls=%async_computation | async-start | bytes 2097152 | tf_op jit(solution)/shard_map/all_to_all | solution.py:246
  7.4 15.1 %all-to-all-done = bf16[4,128,1024]{2,1,0:T(8,128)(2,1)} async-done(((bf16[4,128,1024]{2,1,0:T(8,128)(2,1)}), bf16[4,128,1024]{2,1,0:T(8,128)(2,1)}, u32[]{:S(2)}, u32[]{:S(2)}) %all-to-all-start) | async-done | bytes 1048608 | tf_op jit(solution)/shard_map/all_to_all | solution.py:246
  22.5 2.9 %convolution_convert_fusion = bf16[256,1536]{1,0:T(8,128)(2,1)} fusion(bf16[1536,1024]{1,0:T(8,128)(2,1)S(1)} %copy-done, bf16[512,1024]{1,0:T(8,128)(2,1)} %bitcast.2.refs_0_, s32[]{:T(128)S(6)} %select_n.15), kind=kOutput, calls=%fused_computation | convolution fusion | flops 805699584 | bytes 4456452 | tf_op jit(solution)/shard_map/dot_general | solution.py:19
  25.5 2.6 %collective-permute-done = bf16[256,1536]{1,0:T(8,128)(2,1)} collective-permute-done((bf16[256,1536]{1,0:T(8,128)(2,1)}, bf16[256,1536]{1,0:T(8,128)(2,1)}, u32[]{:S(2)}, u32[]{:S(2)}) %collective-permute-start) | collective-permute-done | bytes 786464 | tf_op jit(solution)/shard_map/ppermute | solution.py:290
  28.1 2.3 %add_convert_fusion.1 = bf16[256,1536]{1,0:T(8,128)(2,1)S(1)} fusion(bf16[256,1536]{1,0:T(8,128)(2,1)} %collective-permute-done, bf16[1536,1024]{1,0:T(8,128)(2,1)S(1)} %copy-done, bf16[512,1024]{1,0:T(8,128)(2,1)} %bitcast.2.refs_0_, s32[]{:T(128)S(6)} %select_n.14), kind=kOutput, calls=%fused_computation.2 | convolution fusion | flops 806486016 | bytes 5242884 | tf_op jit(solution)/shard_map/dot_general | solution.py:19
  30.5 2.0 %collective-permute-start.4 = (bf16[128,1536]{1,0:T(8,128)(2,1)}, bf16[128,1536]{1,0:T(8,128)(2,1)}, u32[]{:S(2)}, u32[]{:S(2)}) collective-permute-start(bf16[128,1536]{1,0:T(8,128)(2,1)} %refs_0_), channel_id=1, source_target_pairs={{0,2},{1,3},{2,0},{3,1},{4,6},{5,7},{6,4},{7,5},{8,10},{9,11},{10,... | collective-permute-start | bytes 1179656 | tf_op jit(solution)/shard_map/ppermute | solution.py:254
  32.6 18.3 %collective-permute-done.1 = bf16[256,1536]{1,0:T(8,128)(2,1)S(1)} collective-permute-done((bf16[256,1536]{1,0:T(8,128)(2,1)S(1)}, bf16[256,1536]{1,0:T(8,128)(2,1)S(1)}, u32[]{:S(2)}, u32[]{:S(2)}) %collective-permute-start.1) | collective-permute-done | bytes 786464 | tf_op jit(solution)/shard_map/ppermute | solution.py:294
  50.9 1.1 add_convert_fusion.mine
  52.5 6.9 %collective-permute-done.4.refs_2_ = bf16[128,1536]{1,0:T(8,128)(2,1)} collective-permute-done((bf16[128,1536]{1,0:T(8,128)(2,1)}, bf16[128,1536]{1,0:T(8,128)(2,1)}, u32[]{:S(2)}, u32[]{:S(2)}) %collective-permute-start.4) | collective-permute-done | bytes 393248 | tf_op jit(solution)/shard_map/ppermute | solution.py:254
  59.4 7.6 %collective-permute-done.7.refs_6_ = bf16[128,1536]{1,0:T(8,128)(2,1)} collective-permute-done((bf16[128,1536]{1,0:T(8,128)(2,1)}, bf16[128,1536]{1,0:T(8,128)(2,1)}, u32[]{:S(2)}, u32[]{:S(2)}) %collective-permute-start.7) | collective-permute-done | bytes 393248 | tf_op jit(solution)/shard_map/ppermute | solution.py:254
  67.1 1.9 %collective-permute-done.8.refs_7_ = bf16[128,1536]{1,0:T(8,128)(2,1)} collective-permute-done((bf16[128,1536]{1,0:T(8,128)(2,1)}, bf16[128,1536]{1,0:T(8,128)(2,1)}, u32[]{:S(2)}, u32[]{:S(2)}) %collective-permute-start.8) | collective-permute-done | bytes 393248 | tf_op jit(solution)/shard_map/ppermute | solution.py:256
  69.1 9.1 %shard_map.202 = (bf16[512,1536]{1,0:T(8,128)(2,1)}, f32[512,1536]{1,0:T(8,128)}, f32[512,1536]{1,0:T(8,128)}, bf16[512,1536]{1,0:T(8,128)(2,1)}, bf16[512,1536]{1,0:T(8,128)(2,1)}) custom-call(s32[4]{0:T(128)S(1)} %pad_add_fusion.places, bf16[128,1536]{1,0:T(8,128)(2,1)} %refs_0_, bf16[128,1536]{1,0:T(8,128)(2,1)} %collective-permute-done.3.refs_1_, ...), custom_call_target="tpu_custom_call" | custom-call | flops 47185920 | bytes 184320 | tf_op jit(solution)/shard_map/pallas_call | solution.py:269
  78.2 7.4 %shard_map.205 = (f32[1536,1024]{1,0:T(8,128)}, f32[1,1536]{1,0:T(1,128)S(1)}) custom-call(bf16[512,1536]{1,0:T(8,128)(2,1)} %get-tuple-element.42.left, bf16[512,1024]{1,0:T(8,128)(2,1)} %bitcast.2.refs_0_), custom_call_target="tpu_custom_call" | custom-call | flops 1610612736 | bytes 6291456 | tf_op jit(solution)/shard_map/pallas_call | solution.py:198
  86.2 3.3 %all-to-all-start.4 = ((f32[4,1,1536]{2,1,0:T(1,128)}), f32[4,1,1536]{2,1,0:T(1,128)S(1)}, u32[]{:S(2)}, u32[]{:S(2)}) async-start(f32[4,1,1536]{2,1,0:T(1,128)} %broadcast_in_dim.5), calls=%async_computation.4 | async-start | bytes 49152 | tf_op jit(solution)/shard_map/all_to_all | solution.py:39
  89.5 14.1 %shard_map.203 = (bf16[512,1536]{1,0:T(8,128)(2,1)}, bf16[512,1536]{1,0:T(8,128)(2,1)}, f32[8,1536]{1,0:T(8,128)S(1)}, bf16[8,64,1024]{2,1,0:T(8,128)(2,1)}) custom-call(s32[1]{0:T(128)} %bitcast.core, bf16[256,1536]{1,0:T(8,128)(2,1)} %add_convert_fusion.mine, bf16[256,1536]{1,0:T(8,128)(2,1)} %collective-permute-done.2.theirs, ...), custom_call_target="tpu_custom_call" | custom-call | flops 3221225472 | bytes 12582912 | tf_op jit(solution)/shard_map/pallas_call | solution.py:307
  103.6 0.8 multiply_reduce_fusion
  104.4 9.1 %shard_map.204 = (f32[1024,1536]{1,0:T(8,128)}, f32[1024,1536]{1,0:T(8,128)}, f32[1,1024]{1,0:T(1,128)S(1)}, f32[1,1024]{1,0:T(1,128)S(1)}) custom-call(bf16[512,1024]{1,0:T(8,128)(2,1)} %left.1, bf16[512,1536]{1,0:T(8,128)(2,1)} %get-tuple-element.38.refs_0_, bf16[512,1536]{1,0:T(8,128)(2,1)} %get-tuple-element.39.refs_1_), custom_call_target="tpu_custom_call" | custom-call | flops 3221225472 | bytes 12582912 | tf_op jit(solution)/shard_map/pallas_call | solution.py:198
  113.6 13.4 %all_to_all.27 = f32[8,1,2054]{2,1,0:T(1,128)S(1)} all-to-all(f32[8,1,2054]{2,1,0:T(1,128)S(1)} %broadcast_in_dim.4), channel_id=1, replica_groups=mesh['fs'=8,'tp'=4] {'fs'}, dimensions={0} | all-to-all | bytes 131456 | tf_op jit(solution)/shard_map/all_to_all | solution.py:39
  127.0 4.2 %all-to-all-start.1 = ((bf16[8,64,1024]{2,1,0:T(8,128)(2,1)}), bf16[8,64,1024]{2,1,0:T(8,128)(2,1)}, u32[]{:S(2)}, u32[]{:S(2)}) async-start(bf16[8,64,1024]{2,1,0:T(8,128)(2,1)} %get-tuple-element.37), calls=%async_computation.1 | async-start | bytes 2097152 | tf_op jit(solution)/shard_map/all_to_all | solution.py:342
  132.5 24.1 %all-to-all-done.1 = bf16[8,64,1024]{2,1,0:T(8,128)(2,1)} async-done(((bf16[8,64,1024]{2,1,0:T(8,128)(2,1)}), bf16[8,64,1024]{2,1,0:T(8,128)(2,1)}, u32[]{:S(2)}, u32[]{:S(2)}) %all-to-all-start.1) | async-done | bytes 1048608 | tf_op jit(solution)/shard_map/all_to_all | solution.py:342
  156.6 2.1 %reduce_sum.48 = bf16[64,1024]{1,0:T(8,128)(2,1)} reduce(bf16[8,64,1024]{2,1,0:T(8,128)(2,1)} %all-to-all-done.1, bf16[]{:T(256)} %constant.27.clone.1), dimensions={0}, to_apply=%region_0.1 | reduce | flops 458752 | bytes 1179650 | tf_op jit(solution)/shard_map/reduce_sum | solution.py:356
  158.7 3.3 %all-to-all-start.2 = ((bf16[4,16,1024]{2,1,0:T(8,128)(2,1)}), bf16[4,16,1024]{2,1,0:T(8,128)(2,1)S(1)}, u32[]{:S(2)}, u32[]{:S(2)}) async-start(bf16[4,16,1024]{2,1,0:T(8,128)(2,1)} %bitcast.7), calls=%async_computation.2 | async-start | bytes 262144 | tf_op jit(solution)/shard_map/all_to_all | solution.py:357
  163.3 3.3 %all-to-all-done.2 = bf16[4,16,1024]{2,1,0:T(8,128)(2,1)S(1)} async-done(((bf16[4,16,1024]{2,1,0:T(8,128)(2,1)}), bf16[4,16,1024]{2,1,0:T(8,128)(2,1)S(1)}, u32[]{:S(2)}, u32[]{:S(2)}) %all-to-all-start.2) | async-done | bytes 131104 | tf_op jit(solution)/shard_map/all_to_all | solution.py:357
  (39 shorter events, 4.8 us)
Async XLA Ops:
  0.6 21.9 %copy-start = (bf16[1536,1024]{1,0:T(8,128)(2,1)S(1)}, bf16[1536,1024]{1,0:T(8,128)(2,1)}, u32[]{:S(2)}) copy-start(bf16[1536,1024]{1,0:T(8,128)(2,1)} %param.17) | copy-start | bytes 9437188
  3.1 19.4 %all-to-all-start = ((bf16[4,128,1024]{2,1,0:T(8,128)(2,1)}), bf16[4,128,1024]{2,1,0:T(8,128)(2,1)}, u32[]{:S(2)}, u32[]{:S(2)}) async-start(bf16[4,128,1024]{2,1,0:T(8,128)(2,1)} %bitcast.25), calls=%async_computation | async-start | bytes 2097152 | tf_op jit(solution)/shard_map/all_to_all | solution.py:246
  25.4 2.6 %collective-permute-start = (bf16[256,1536]{1,0:T(8,128)(2,1)}, bf16[256,1536]{1,0:T(8,128)(2,1)}, u32[]{:S(2)}, u32[]{:S(2)}) collective-permute-start(bf16[256,1536]{1,0:T(8,128)(2,1)} %convolution_convert_fusion), channel_id=1, source_target_pairs={{0,1},{1,0},{2,3},{3,2},{4,5},{5,4},{6,7},{7,6},{8,9},{9,8},{10,11... | collective-permute-start | bytes 2359304 | tf_op jit(solution)/shard_map/ppermute | solution.py:290
  25.5 41.6 %copy-start.3 = (bf16[1536]{0:T(1024)(128)(2,1)S(1)}, bf16[1536]{0:T(1024)(128)(2,1)}, u32[]{:S(2)}) copy-start(bf16[1536]{0:T(1024)(128)(2,1)} %param.20) | copy-start | bytes 9220
  25.5 41.6 %copy-start.4 = (bf16[1536]{0:T(1024)(128)(2,1)S(1)}, bf16[1536]{0:T(1024)(128)(2,1)}, u32[]{:S(2)}) copy-start(bf16[1536]{0:T(1024)(128)(2,1)} %param.21) | copy-start | bytes 9220
  25.5 43.6 %copy-start.1 = (bf16[3,1536]{1,0:T(4,128)(2,1)S(1)}, bf16[3,1536]{1,0:T(4,128)(2,1)}, u32[]{:S(2)}) copy-start(bf16[3,1536]{1,0:T(4,128)(2,1)} %conv_act.1) | copy-start | bytes 27652
  25.5 43.6 %copy-start.2 = (bf16[3,1536]{1,0:T(4,128)(2,1)S(1)}, bf16[3,1536]{1,0:T(4,128)(2,1)}, u32[]{:S(2)}) copy-start(bf16[3,1536]{1,0:T(4,128)(2,1)} %conv_val.1) | copy-start | bytes 27652
  30.4 20.5 %collective-permute-start.1 = (bf16[256,1536]{1,0:T(8,128)(2,1)S(1)}, bf16[256,1536]{1,0:T(8,128)(2,1)S(1)}, u32[]{:S(2)}, u32[]{:S(2)}) collective-permute-start(bf16[256,1536]{1,0:T(8,128)(2,1)S(1)} %add_convert_fusion.1), channel_id=1, source_target_pairs={{0,2},{1,3},{2,0},{3,1},{4,6},{5,7},{6,4},{7,5},{8,10},{9,11},{10,... | collective-permute-start | bytes 2359304 | tf_op jit(solution)/shard_map/ppermute | solution.py:294
  30.5 28.9 %collective-permute-start.4 = (bf16[128,1536]{1,0:T(8,128)(2,1)}, bf16[128,1536]{1,0:T(8,128)(2,1)}, u32[]{:S(2)}, u32[]{:S(2)}) collective-permute-start(bf16[128,1536]{1,0:T(8,128)(2,1)} %refs_0_), channel_id=1, source_target_pairs={{0,2},{1,3},{2,0},{3,1},{4,6},{5,7},{6,4},{7,5},{8,10},{9,11},{10,... | collective-permute-start | bytes 1179656 | tf_op jit(solution)/shard_map/ppermute | solution.py:254
  32.5 34.5 %collective-permute-start.7 = (bf16[128,1536]{1,0:T(8,128)(2,1)}, bf16[128,1536]{1,0:T(8,128)(2,1)}, u32[]{:S(2)}, u32[]{:S(2)}) collective-permute-start(bf16[128,1536]{1,0:T(8,128)(2,1)} %refs_4_), channel_id=1, source_target_pairs={{0,2},{1,3},{2,0},{3,1},{4,6},{5,7},{6,4},{7,5},{8,10},{9,11},{10,... | collective-permute-start | bytes 1179656 | tf_op jit(solution)/shard_map/ppermute | solution.py:254
  52.0 37.5 %collective-permute-start.2 = (bf16[256,1536]{1,0:T(8,128)(2,1)}, bf16[256,1536]{1,0:T(8,128)(2,1)}, u32[]{:S(2)}, u32[]{:S(2)}) collective-permute-start(bf16[256,1536]{1,0:T(8,128)(2,1)} %add_convert_fusion.mine), channel_id=1, source_target_pairs={{0,1},{1,0},{2,3},{3,2},{4,5},{5,4},{6,7},{7,6},{8,9},{9,8},{10,11... | collective-permute-start | bytes 2359304 | tf_op jit(solution)/shard_map/ppermute | solution.py:300
  52.0 15.2 %collective-permute-start.3 = (bf16[128,1536]{1,0:T(8,128)(2,1)}, bf16[128,1536]{1,0:T(8,128)(2,1)}, u32[]{:S(2)}, u32[]{:S(2)}) collective-permute-start(bf16[128,1536]{1,0:T(8,128)(2,1)} %refs_0_), channel_id=1, source_target_pairs={{0,1},{1,0},{2,3},{3,2},{4,5},{5,4},{6,7},{7,6},{8,9},{9,8},{10,11... | collective-permute-start | bytes 1179656 | tf_op jit(solution)/shard_map/ppermute | solution.py:255
  52.5 14.7 %collective-permute-start.6 = (bf16[128,1536]{1,0:T(8,128)(2,1)}, bf16[128,1536]{1,0:T(8,128)(2,1)}, u32[]{:S(2)}, u32[]{:S(2)}) collective-permute-start(bf16[128,1536]{1,0:T(8,128)(2,1)} %refs_4_), channel_id=1, source_target_pairs={{0,1},{1,0},{2,3},{3,2},{4,5},{5,4},{6,7},{7,6},{8,9},{9,8},{10,11... | collective-permute-start | bytes 1179656 | tf_op jit(solution)/shard_map/ppermute | solution.py:255
  59.4 7.7 %collective-permute-start.5 = (bf16[128,1536]{1,0:T(8,128)(2,1)}, bf16[128,1536]{1,0:T(8,128)(2,1)}, u32[]{:S(2)}, u32[]{:S(2)}) collective-permute-start(bf16[128,1536]{1,0:T(8,128)(2,1)} %collective-permute-done.4.refs_2_), channel_id=1, source_target_pairs={{0,1},{1,0},{2,3},{3,2},{4,5},{5,4},{6,7},{7,6},{8,9},{9,8},{10,11... | collective-permute-start | bytes 1179656 | tf_op jit(solution)/shard_map/ppermute | solution.py:256
  67.0 2.1 %collective-permute-start.8 = (bf16[128,1536]{1,0:T(8,128)(2,1)}, bf16[128,1536]{1,0:T(8,128)(2,1)}, u32[]{:S(2)}, u32[]{:S(2)}) collective-permute-start(bf16[128,1536]{1,0:T(8,128)(2,1)} %collective-permute-done.7.refs_6_), channel_id=1, source_target_pairs={{0,1},{1,0},{2,3},{3,2},{4,5},{5,4},{6,7},{7,6},{8,9},{9,8},{10,11... | collective-permute-start | bytes 1179656 | tf_op jit(solution)/shard_map/ppermute | solution.py:256
  86.2 27.4 %all-to-all-start.4 = ((f32[4,1,1536]{2,1,0:T(1,128)}), f32[4,1,1536]{2,1,0:T(1,128)S(1)}, u32[]{:S(2)}, u32[]{:S(2)}) async-start(f32[4,1,1536]{2,1,0:T(1,128)} %broadcast_in_dim.5), calls=%async_computation.4 | async-start | bytes 49152 | tf_op jit(solution)/shard_map/all_to_all | solution.py:39
  127.0 29.7 %all-to-all-start.1 = ((bf16[8,64,1024]{2,1,0:T(8,128)(2,1)}), bf16[8,64,1024]{2,1,0:T(8,128)(2,1)}, u32[]{:S(2)}, u32[]{:S(2)}) async-start(bf16[8,64,1024]{2,1,0:T(8,128)(2,1)} %get-tuple-element.37), calls=%async_computation.1 | async-start | bytes 2097152 | tf_op jit(solution)/shard_map/all_to_all | solution.py:342
  158.7 7.9 %all-to-all-start.2 = ((bf16[4,16,1024]{2,1,0:T(8,128)(2,1)}), bf16[4,16,1024]{2,1,0:T(8,128)(2,1)S(1)}, u32[]{:S(2)}, u32[]{:S(2)}) async-start(bf16[4,16,1024]{2,1,0:T(8,128)(2,1)} %bitcast.7), calls=%async_computation.2 | async-start | bytes 262144 | tf_op jit(solution)/shard_map/all_to_all | solution.py:357
